TPU v7x, 32 devices: a whole 2x2x4 slice. The times are simulated.
32 devices in a mesh: gr: 2 (over core), fs: 8 (over z, y), tp: 2 (over x).
Axes of the slice: x: 2, y: 2, z: 4, core: 2. Of those that a mesh axis runs over, the one named last changes fastest.
Arguments:
- tokens: bfloat16 [6144, 2048], P(('gr', 'fs')), may hold values from -6 to 6
- route_ids: int32 [6144, 2], P(('gr', 'fs')), may hold values from 0 to 7, as said below
- route_weights: float32 [6144, 2], P(('gr', 'fs')), may hold values from 0.1 to 1
- norm_gain: float32 [2048], P(('gr', 'fs')), may hold values from 0.1 to 1.9
- gate_weight: float32 [8, 2048, 1024], P(None, ('gr', 'fs'), 'tp'), may hold values from -0.125 to 0.125
- up_weight: float32 [8, 2048, 1024], P(None, ('gr', 'fs'), 'tp'), may hold values from -0.125 to 0.125
- down_weight: float32 [8, 1024, 2048], P(None, ('gr', 'fs'), 'tp'), may hold values from -0.1875 to 0.1875
Outputs:
- gate_new: bfloat16 [8, 2048, 1024], P('fs', None, 'tp')
- up_new: bfloat16 [8, 2048, 1024], P('fs', None, 'tp')
- down_new: bfloat16 [8, 1024, 2048], P('fs', 'tp')
- mixed: bfloat16 [6144, 2048], P(('gr', 'fs'), 'tp')
Inputs may be any that keep to these rules, and one draw needn't show every extreme that they name: `route_ids`: each row names two different experts of one group (expert e belongs to group e // 2); in each device's block of 384 rows every expert is named by exactly 96 rows.
All inputs are finite; a program needn't handle non-finite values.
Results may differ from a plain program's by a relative error of at most 0.015.
Values may be sent and summed in bfloat16 or wider, within the bound.
A program may use at most 64 MiB of HBM per device.

v0:
```python
import jax
import jax.numpy as jnp
from jax import lax
from jax.sharding import PartitionSpec as P


def local(tokens, route_ids, route_weights, norm_gain, gate_weight, up_weight, down_weight):
    gate_folded = (gate_weight * norm_gain[None, :, None]).astype(jnp.bfloat16)
    up_folded = (up_weight * norm_gain[None, :, None]).astype(jnp.bfloat16)
    down_rounded = down_weight.astype(jnp.bfloat16)
    moved = (
        lax.all_to_all(gate_folded, "fs", split_axis=0, concat_axis=1, tiled=True),
        lax.all_to_all(up_folded, "fs", split_axis=0, concat_axis=1, tiled=True),
        lax.all_to_all(down_rounded, "fs", split_axis=0, concat_axis=1, tiled=True),
    )
    gate_new, up_new, down_whole = (
        lax.all_gather(moved[0], "gr", axis=1, tiled=True),
        lax.all_gather(moved[1], "gr", axis=1, tiled=True),
        lax.all_gather(moved[2], "gr", axis=1, tiled=True),
    )
    down_new = lax.all_to_all(down_whole, "tp", split_axis=1, concat_axis=2, tiled=True)
    tok = tokens.shape[0]
    width = tokens.shape[1]
    experts = gate_weight.shape[0]
    cap = 2 * tok // experts
    flat_ids = route_ids.reshape(-1)
    onehot = (flat_ids[:, None] == jnp.arange(experts, dtype=jnp.int32)[None, :]).astype(jnp.int32)
    slot = jnp.sum(jnp.cumsum(onehot, axis=0) * onehot, axis=1) - 1
    position = flat_ids * cap + slot
    source = (
        jnp.zeros((experts * cap,), jnp.int32)
        .at[position]
        .set(jnp.arange(2 * tok, dtype=jnp.int32) // 2)
    )
    widened = tokens.astype(jnp.float32)
    normed = (
        widened * lax.rsqrt(jnp.mean(widened * widened, axis=-1, keepdims=True) + 1e-06)
    ).astype(jnp.bfloat16)
    outgoing = normed[source].reshape(experts, cap, width)
    received = lax.all_to_all(outgoing, "fs", split_axis=0, concat_axis=0, tiled=True)
    senders, count, _ = received.shape
    rows = received.reshape(senders * count, width)
    first = jnp.dot(rows, gate_new[0], preferred_element_type=jnp.float32)
    second = jnp.dot(rows, up_new[0], preferred_element_type=jnp.float32)
    hidden = (jax.nn.silu(first) * second).astype(jnp.bfloat16)
    partial_out = jnp.dot(hidden, down_new[0], preferred_element_type=jnp.float32)
    summed = lax.psum_scatter(
        partial_out.reshape(senders, count, width).astype(jnp.bfloat16),
        "tp",
        scatter_dimension=2,
        tiled=True,
    )
    returned = lax.all_to_all(summed, "fs", split_axis=0, concat_axis=0, tiled=True)
    columns = returned.shape[2]
    route_out = returned.reshape(experts * cap, columns)[position].reshape(tok, 2, columns)
    mixed = jnp.sum(route_weights[:, :, None] * route_out.astype(jnp.float32), axis=1).astype(
        jnp.bfloat16
    )
    return (gate_new, up_new, down_new, mixed)


def solution(mesh):
    placed = (
        P(("gr", "fs"), None),
        P(("gr", "fs"), None),
        P(("gr", "fs"), None),
        P(("gr", "fs")),
        P(None, ("gr", "fs"), "tp"),
        P(None, ("gr", "fs"), "tp"),
        P(None, ("gr", "fs"), "tp"),
    )
    return jax.shard_map(
        local,
        mesh=mesh,
        in_specs=placed,
        out_specs=(
            P("fs", None, "tp"),
            P("fs", None, "tp"),
            P("fs", "tp", None),
            P(("gr", "fs"), "tp"),
        ),
        check_vma=False,
    )
```

profile of v0, /device:TPU:0, one launch (start us, length us, event | category | flops | bytes accessed | tf_op | source)
XLA Modules:
  0.0 330.1 jit_solution(6184814864289709541)
XLA Ops:
  9.9 7.3 %all-to-all-start.2 = ((bf16[8,64,1024]{2,1,0:T(8,128)(2,1)}), bf16[8,64,1024]{2,1,0:T(8,128)(2,1)S(1)}, u32[]{:S(2)}, u32[]{:S(2)}) async-start(bf16[8,64,1024]{2,1,0:T(8,128)(2,1)} %convert_element_type.37), calls=%async_computation.2 | async-start | bytes 2097152 | tf_op jit(solution)/shard_map/all_to_all | solution.py:14
  17.2 4.2 %multiply_convert_fusion = (bf16[8,128,512]{2,1,0:T(8,128)(2,1)}, bf16[8,128,512]{2,1,0:T(8,128)(2,1)}) fusion(f32[8,128,512]{2,1,0:T(8,128)} %param.12, f32[128]{0:T(128)S(1)} %copy-done.9, f32[8,128,512]{2,1,0:T(8,128)} %param.11), kind=kLoop, calls=%fused_computation.13 | loop fusion | flops 2097152 | bytes 6291968 | tf_op jit(solution)/shard_map/convert_element_type | solution.py:9
  21.4 21.6 %all-to-all-done.2 = bf16[8,64,1024]{2,1,0:T(8,128)(2,1)S(1)} async-done(((bf16[8,64,1024]{2,1,0:T(8,128)(2,1)}), bf16[8,64,1024]{2,1,0:T(8,128)(2,1)S(1)}, u32[]{:S(2)}, u32[]{:S(2)}) %all-to-all-start.2) | async-done | bytes 1048608 | tf_op jit(solution)/shard_map/all_to_all | solution.py:14
  43.0 3.6 %all-to-all-start = ((bf16[8,128,512]{2,1,0:T(8,128)(2,1)}), bf16[8,128,512]{2,1,0:T(8,128)(2,1)S(1)}, u32[]{:S(2)}, u32[]{:S(2)}) async-start(bf16[8,128,512]{2,1,0:T(8,128)(2,1)} %get-tuple-element.17), calls=%async_computation | async-start | bytes 2097152 | tf_op jit(solution)/shard_map/all_to_all | solution.py:12
  47.3 25.2 %all-to-all-done = bf16[8,128,512]{2,1,0:T(8,128)(2,1)S(1)} async-done(((bf16[8,128,512]{2,1,0:T(8,128)(2,1)}), bf16[8,128,512]{2,1,0:T(8,128)(2,1)S(1)}, u32[]{:S(2)}, u32[]{:S(2)}) %all-to-all-start) | async-done | bytes 1048608 | tf_op jit(solution)/shard_map/all_to_all | solution.py:12
  72.5 4.2 %all-to-all-start.1 = ((bf16[8,128,512]{2,1,0:T(8,128)(2,1)}), bf16[8,128,512]{2,1,0:T(8,128)(2,1)}, u32[]{:S(2)}, u32[]{:S(2)}) async-start(bf16[8,128,512]{2,1,0:T(8,128)(2,1)} %get-tuple-element.16), calls=%async_computation.1 | async-start | bytes 2097152 | tf_op jit(solution)/shard_map/all_to_all | solution.py:13
  83.3 6.8 %copy.51 = bf16[1,1024,1024]{2,0,1:T(2,128)(2,1)} copy(bf16[1,1024,1024]{2,1,0:T(8,128)(2,1)} %all-gather.8.cloned.1.call-done) | data formatting | bytes 4194304 | tf_op jit(solution)/shard_map/all_gather | solution.py:19
  90.6 12.8 %reduce.2 = bf16[1024,1024]{1,0:T(8,128)(2,1)S(1)} reduce(bf16[1024,1,1024]{2,1,0:T(2,128)(2,1)} %bitcast.38, bf16[]{:T(256)} %broadcast.104), dimensions={1}, to_apply=%bitcast.33.reduce_sub_computation | reduce | bytes 4194306
  105.9 5.0 %all-to-all-start.3 = ((bf16[2,2,262144]{2,1,0:T(2,128)(2,1)}), bf16[2,2,262144]{2,1,0:T(2,128)(2,1)}, u32[]{:S(2)}, u32[]{:S(2)}) async-start(bf16[2,2,262144]{2,1,0:T(2,128)(2,1)} %reshape.128), calls=%async_computation.3 | async-start | bytes 4194304 | tf_op jit(solution)/shard_map/all_to_all | solution.py:21
  111.6 4.3 %gather_fusion = bf16[768,2048]{1,0:T(8,128)(2,1)} fusion(bf16[384,2048]{1,0:T(8,128)(2,1)S(1)} %fusion.1, s32[1024]{0:T(1024)S(1)} %pad_clamp_fusion.1), kind=kCustom, calls=%fused_computation | custom fusion | bytes 6294528 | tf_op jit(solution)/shard_map/gather | solution.py:39
  115.9 19.5 %all-to-all-done.3 = bf16[2,2,262144]{2,1,0:T(2,128)(2,1)} async-done(((bf16[2,2,262144]{2,1,0:T(2,128)(2,1)}), bf16[2,2,262144]{2,1,0:T(2,128)(2,1)}, u32[]{:S(2)}, u32[]{:S(2)}) %all-to-all-start.3) | async-done | bytes 2097184 | tf_op jit(solution)/shard_map/all_to_all | solution.py:21
  135.3 5.7 %all-to-all-start.4 = ((bf16[8,96,2048]{2,1,0:T(8,128)(2,1)}), bf16[8,96,2048]{2,1,0:T(8,128)(2,1)}, u32[]{:S(2)}, u32[]{:S(2)}) async-start(bf16[8,96,2048]{2,1,0:T(8,128)(2,1)} %bitcast.40), calls=%async_computation.4 | async-start | bytes 6291456 | tf_op jit(solution)/shard_map/all_to_all | solution.py:40
  142.7 4.3 %reshape.129 = bf16[1024,1,1024]{2,1,0:T(2,128)(2,1)} reshape(bf16[2,2,262144]{2,1,0:T(2,128)(2,1)} %all-to-all-done.3) | data formatting | bytes 4194304
  156.3 53.8 %all-to-all-done.4 = bf16[8,96,2048]{2,1,0:T(8,128)(2,1)} async-done(((bf16[8,96,2048]{2,1,0:T(8,128)(2,1)}), bf16[8,96,2048]{2,1,0:T(8,128)(2,1)}, u32[]{:S(2)}, u32[]{:S(2)}) %all-to-all-start.4) | async-done | bytes 3145760 | tf_op jit(solution)/shard_map/all_to_all | solution.py:40
  210.1 5.5 %fusion.4 = f32[768,512]{1,0:T(8,128)} fusion(bf16[768,2048]{1,0:T(8,128)(2,1)} %bitcast.9, bf16[1,2048,512]{2,1,0:T(8,128)(2,1)} %all-gather.4.cloned.1.call-done), kind=kOutput, calls=%fused_computation.11 | convolution fusion | flops 1610612736 | bytes 6815744 | tf_op jit(solution)/shard_map/dot_general | solution.py:43
  215.6 5.1 %multiply_convert_fusion.2 = bf16[768,512]{1,0:T(8,128)(2,1)S(1)} fusion(f32[768,512]{1,0:T(8,128)} %fusion.4, bf16[768,2048]{1,0:T(8,128)(2,1)} %bitcast.9, bf16[1,2048,512]{2,1,0:T(8,128)(2,1)} %all-gather.6.cloned.1.call-done), kind=kOutput, calls=%fused_computation.15 | convolution fusion | flops 1612972032 | bytes 7602176 | tf_op jit(solution)/shard_map/dot_general | solution.py:44
  220.6 3.4 %convolution_convert_fusion = bf16[8,96,2048]{2,1,0:T(8,128)(2,1)} fusion(bf16[8,96,512]{2,1,0:T(8,128)(2,1)S(1)} %bitcast.46, bf16[512,2048,1]{1,0,2:T(8,128)(2,1)S(1)} %copy-done.6), kind=kOutput, calls=%fused_computation.5 | convolution fusion | flops 1612185600 | bytes 6029312 | tf_op jit(solution)/shard_map/dot_general | solution.py:46
  224.1 41.7 %reduce-scatter.2.cloned.1.call-done = bf16[8,96,1024]{2,1,0:T(8,128)(2,1)} async-done(((bf16[8,96,2048]{2,1,0:T(8,128)(2,1)}), bf16[8,96,1024]{2,1,0:T(8,128)(2,1)}) %reduce-scatter.2.cloned.1.call-update) | async-done | bytes 1572880 | tf_op jit(solution)/shard_map/reduce_scatter | solution.py:47
  265.8 5.5 %all-to-all-start.5 = ((bf16[8,96,1024]{2,1,0:T(8,128)(2,1)}), bf16[8,96,1024]{2,1,0:T(8,128)(2,1)S(1)}, u32[]{:S(2)}, u32[]{:S(2)}) async-start(bf16[8,96,1024]{2,1,0:T(8,128)(2,1)} %reduce-scatter.2.cloned.1.call-done), calls=%async_computation.6 | async-start | bytes 3145728 | tf_op jit(solution)/shard_map/all_to_all | solution.py:53
  271.5 3.9 %copy.40 = bf16[1,512,2,1024]{1,3,2,0:T(8,128)(2,1)} copy(bf16[1,512,2,1024]{3,1,2,0:T(8,128)(2,1)} %bitcast.37) | data formatting | bytes 4194304 | tf_op jit(solution)/shard_map/all_to_all | solution.py:21
  275.4 3.9 %copy.48 = bf16[1,512,2048]{2,1,0:T(8,128)(2,1)} copy(bf16[1,512,2048]{1,2,0:T(8,128)(2,1)} %bitcast.41) | data formatting | bytes 4194304
  279.4 28.8 %all-to-all-done.5 = bf16[8,96,1024]{2,1,0:T(8,128)(2,1)S(1)} async-done(((bf16[8,96,1024]{2,1,0:T(8,128)(2,1)}), bf16[8,96,1024]{2,1,0:T(8,128)(2,1)S(1)}, u32[]{:S(2)}, u32[]{:S(2)}) %all-to-all-start.5) | async-done | bytes 1572896 | tf_op jit(solution)/shard_map/all_to_all | solution.py:53
  308.2 3.5 %gather_fusion.1 = bf16[768,1024]{1,0:T(8,128)(2,1)} fusion(bf16[768,1024]{1,0:T(8,128)(2,1)S(1)} %bitcast.35, s32[1024]{0:T(1024)S(1)} %pad_clamp_fusion), kind=kCustom, calls=%fused_computation.1 | custom fusion | bytes 3148800 | tf_op jit(solution)/shard_map/gather | solution.py:55
  315.1 4.8 %multiply_reduce_fusion = bf16[384,1024]{1,0:T(8,128)(2,1)} fusion(f32[384,2,1024]{2,1,0:T(2,128)S(1)} %reshape.97, f32[384,2]{1,0:T(8,128)S(1)} %copy.41), kind=kLoop, calls=%fused_computation.8 | loop fusion | flops 1179648 | bytes 3935232 | tf_op jit(solution)/shard_map/reduce_sum | solution.py:56
  (65 shorter events, 31.8 us)
Async XLA Ops:
  7.2 10.1 %copy-start.9 = (f32[128]{0:T(128)S(1)}, f32[128]{0:T(128)}, u32[]{:S(2)}) copy-start(f32[128]{0:T(128)} %param.10) | copy-start | bytes 1540
  9.9 33.1 %all-to-all-start.2 = ((bf16[8,64,1024]{2,1,0:T(8,128)(2,1)}), bf16[8,64,1024]{2,1,0:T(8,128)(2,1)S(1)}, u32[]{:S(2)}, u32[]{:S(2)}) async-start(bf16[8,64,1024]{2,1,0:T(8,128)(2,1)} %convert_element_type.37), calls=%async_computation.2 | async-start | bytes 2097152 | tf_op jit(solution)/shard_map/all_to_all | solution.py:14
  43.0 3.6 %copy-start.3 = (bf16[8,64,1024]{2,1,0:T(8,128)(2,1)}, bf16[8,64,1024]{2,1,0:T(8,128)(2,1)S(1)}, u32[]{:S(2)}) copy-start(bf16[8,64,1024]{2,1,0:T(8,128)(2,1)S(1)} %all-to-all-done.2) | copy-start | bytes 3145732
  43.0 29.5 %all-to-all-start = ((bf16[8,128,512]{2,1,0:T(8,128)(2,1)}), bf16[8,128,512]{2,1,0:T(8,128)(2,1)S(1)}, u32[]{:S(2)}, u32[]{:S(2)}) async-start(bf16[8,128,512]{2,1,0:T(8,128)(2,1)} %get-tuple-element.17), calls=%async_computation | async-start | bytes 2097152 | tf_op jit(solution)/shard_map/all_to_all | solution.py:12
  46.6 30.2 %copy-start.7 = (s32[384,2]{0,1:T(2,128)S(1)}, s32[384,2]{0,1:T(2,128)}, u32[]{:S(2)}) copy-start(s32[384,2]{0,1:T(2,128)} %param.8) | copy-start | bytes 9220
  46.6 36.7 %all-gather.8.cloned.1.call-start = ((), (), s32[]{:S(2)}) async-start(), calls=%async_computation.9 | async-start | bytes 3145728 | tf_op jit(solution)/shard_map/all_gather | solution.py:19
  72.5 17.5 %copy-start.2 = (bf16[8,128,512]{2,1,0:T(8,128)(2,1)}, bf16[8,128,512]{2,1,0:T(8,128)(2,1)S(1)}, u32[]{:S(2)}) copy-start(bf16[8,128,512]{2,1,0:T(8,128)(2,1)S(1)} %all-to-all-done) | copy-start | bytes 3145732
  72.5 33.3 %all-to-all-start.1 = ((bf16[8,128,512]{2,1,0:T(8,128)(2,1)}), bf16[8,128,512]{2,1,0:T(8,128)(2,1)}, u32[]{:S(2)}, u32[]{:S(2)}) async-start(bf16[8,128,512]{2,1,0:T(8,128)(2,1)} %get-tuple-element.16), calls=%async_computation.1 | async-start | bytes 2097152 | tf_op jit(solution)/shard_map/all_to_all | solution.py:13
  105.9 5.0 %copy-start.1 = (bf16[384,2048]{1,0:T(8,128)(2,1)S(1)}, bf16[384,2048]{1,0:T(8,128)(2,1)}, u32[]{:S(2)}) copy-start(bf16[384,2048]{1,0:T(8,128)(2,1)} %param.7) | copy-start | bytes 4718596
  105.9 29.4 %all-to-all-start.3 = ((bf16[2,2,262144]{2,1,0:T(2,128)(2,1)}), bf16[2,2,262144]{2,1,0:T(2,128)(2,1)}, u32[]{:S(2)}, u32[]{:S(2)}) async-start(bf16[2,2,262144]{2,1,0:T(2,128)(2,1)} %reshape.128), calls=%async_computation.3 | async-start | bytes 4194304 | tf_op jit(solution)/shard_map/all_to_all | solution.py:21
  135.3 74.8 %all-to-all-start.4 = ((bf16[8,96,2048]{2,1,0:T(8,128)(2,1)}), bf16[8,96,2048]{2,1,0:T(8,128)(2,1)}, u32[]{:S(2)}, u32[]{:S(2)}) async-start(bf16[8,96,2048]{2,1,0:T(8,128)(2,1)} %bitcast.40), calls=%async_computation.4 | async-start | bytes 6291456 | tf_op jit(solution)/shard_map/all_to_all | solution.py:40
  141.0 15.3 %all-gather.4.cloned.1.call-start = ((), (), s32[]{:S(2)}) async-start(), calls=%async_computation.7 | async-start | bytes 3145728 | tf_op jit(solution)/shard_map/all_gather | solution.py:17
  141.8 73.8 %all-gather.6.cloned.1.call-start = ((), (), s32[]{:S(2)}) async-start(), calls=%async_computation.8 | async-start | bytes 3145728 | tf_op jit(solution)/shard_map/all_gather | solution.py:18
  142.5 123.3 %reduce-scatter.2.cloned.1.call-start = ((), (), s32[]{:S(2)}) async-start(), calls=%async_computation.10 | async-start | bytes 4718592 | tf_op jit(solution)/shard_map/reduce_scatter | solution.py:47
  150.1 1.3 copy-start
  215.6 5.1 %copy-start.6 = (bf16[512,2048,1]{1,0,2:T(8,128)(2,1)S(1)}, bf16[512,2048,1]{1,0,2:T(8,128)(2,1)}, u32[]{:S(2)}) copy-start(bf16[512,2048,1]{1,0,2:T(8,128)(2,1)} %reshape.123) | copy-start | bytes 6291460
  224.1 47.2 %copy-start.8 = (f32[384,2]{0,1:T(2,128)S(1)}, f32[384,2]{0,1:T(2,128)}, u32[]{:S(2)}) copy-start(f32[384,2]{0,1:T(2,128)} %param.9) | copy-start | bytes 9220
  265.8 42.4 %all-to-all-start.5 = ((bf16[8,96,1024]{2,1,0:T(8,128)(2,1)}), bf16[8,96,1024]{2,1,0:T(8,128)(2,1)S(1)}, u32[]{:S(2)}, u32[]{:S(2)}) async-start(bf16[8,96,1024]{2,1,0:T(8,128)(2,1)} %reduce-scatter.2.cloned.1.call-done), calls=%async_computation.6 | async-start | bytes 3145728 | tf_op jit(solution)/shard_map/all_to_all | solution.py:53
  315.1 4.8 %copy-start.4 = (bf16[1,2048,512]{2,1,0:T(8,128)(2,1)S(1)}, bf16[1,2048,512]{2,1,0:T(8,128)(2,1)}, u32[]{:S(2)}) copy-start(bf16[1,2048,512]{2,1,0:T(8,128)(2,1)} %all-gather.4.cloned.1.call-done) | copy-start | bytes 6291460
  319.9 2.3 copy-start.5
Sparse Core Ops, SparseCore 0:
  48.9 11.9 all-gather.7
  144.0 11.0 all-gather.3
  156.6 11.7 all-gather.5
  224.2 41.5 reduce-scatter.1
where the time goes:
time: 331 us; the launch traced here: 330 us
  waiting for transfers between devices  193 us (58%)
  local copies, waits for them, and re-layouts  50.7 us (15%)
  starting transfers between devices  31.7 us (10%)
  other arithmetic  27.2 us (8%)
  matrix products  14 us (4%)
  between operations  14 us (4%)
    all_to_all x1, waiting for transfers between devices, local(): lax.all_to_all(outgoing, 'fs', split_axis=0, concat_axis=0, tiled=True)  53.8 us
    reduce_scatter x1, waiting for transfers between devices, local(): lax.psum_scatter(partial_out.reshape(senders, count, width).astype(jnp.bf...  41.7 us
    all_to_all x1, waiting for transfers between devices, local(): lax.all_to_all(summed, 'fs', split_axis=0, concat_axis=0, tiled=True)  28.8 us
    all_to_all x1, waiting for transfers between devices, local(): lax.all_to_all(gate_folded, 'fs', split_axis=0, concat_axis=1, tiled=True)  25.2 us
    all_to_all x1, waiting for transfers between devices, local(): lax.all_to_all(down_rounded, 'fs', split_axis=0, concat_axis=1, tiled=True)  21.6 us
    unnamed x29, local copies, waits for them, and re-layouts  19.5 us
    all_to_all x1, waiting for transfers between devices, local(): lax.all_to_all(down_whole, 'tp', split_axis=1, concat_axis=2, tiled=True)  19.5 us
    unnamed x1, other arithmetic  12.8 us
  transfers between devices with their start and end apart: 10, of which 6 were waited for; matrix products, arithmetic and copies ran while one was open for 19% of the time, Pallas kernels for 0%

commit v1 on v0

--- a/solution.py
+++ b/solution.py
@@ -1,7 +1,15 @@
+import functools
+
 import jax
 import jax.numpy as jnp
 from jax import lax
+from jax.experimental import pallas as pl
+from jax.experimental.pallas import tpu as pltpu
 from jax.sharding import PartitionSpec as P
+
+GROUPS = 4
+BF16 = jnp.bfloat16
+MESH = pl.DeviceIdType.MESH
 
 
 def local(tokens, route_ids, route_weights, norm_gain, gate_weight, up_weight, down_weight):
@@ -59,6 +67,338 @@
     return (gate_new, up_new, down_new, mixed)
 
 
+def place(n_z, n_y):
+    f = lax.axis_index("fs")
+    return lax.axis_index("gr"), f // n_y, lax.rem(f, n_y), lax.axis_index("tp")
+
+
+def flip(z, k):
+    return (z, z + 1 - 2 * lax.rem(z, 2), lax.rem(z + 2, 4), 3 - z)[k]
+
+
+def device(c, z, y, x, n_y):
+    return {"gr": c, "fs": z * n_y + y, "tp": x}
+
+
+def greet(peers):
+    barrier = pltpu.get_barrier_semaphore()
+    for peer in peers:
+        pl.semaphore_signal(barrier, inc=1, device_id=peer, device_id_type=MESH)
+    pl.semaphore_wait(barrier, len(peers))
+
+
+def remote(src, dst, send, recv, peer):
+    return pltpu.make_async_remote_copy(
+        src_ref=src, dst_ref=dst, send_sem=send, recv_sem=recv,
+        device_id=peer, device_id_type=MESH,
+    )
+
+
+def hand_over(
+    n_z, n_y,
+    gate_in, up_in, down_in, tok_in, rw_in,
+    gate_out, up_out, down_out, rows_out, rw_out,
+    w_send, w_recv, f_send, f_recv,
+    tz_send, tz_recv, ty_send, ty_recv, tx_send, tx_recv,
+    rz_send, rz_recv, ry_send, ry_recv, own, spare,
+):
+    c, z, y, x = place(n_z, n_y)
+    me = z * n_y + y
+    n_fs = n_z * n_y
+    g_rows, d_rows = gate_in.shape[1], down_in.shape[1]
+    half = tok_in.shape[2]
+    dev = functools.partial(device, n_y=n_y)
+    ks = [(kz, ky) for kz in (3, 2, 1, 0) for ky in (1, 0)]
+
+    def peer_of(k):
+        return flip(z, k[0]), (1 - y if k[1] else y)
+
+    other = dev(1 - c, z, y, x)
+    x_nbr = dev(c, z, y, 1 - x)
+    y_nbr = dev(c, z, 1 - y, x)
+    peers = [dev(c, *peer_of(k), x) for k in ks if k != (0, 0)]
+    peers += [dev(x, *peer_of(k), c) for k in ks if k != (0, 0)]
+    peers += [other, x_nbr, dev(1 - c, z, y, 1 - x)]
+    greet(peers)
+
+    def xcols(i):
+        return pl.ds(pl.multiple_of(i * half, half), half)
+
+    def grow(core, src):
+        return pl.ds(pl.multiple_of((core * n_fs + src) * g_rows, g_rows), g_rows)
+
+    def drow(src):
+        return pl.ds(pl.multiple_of(src * d_rows, d_rows), d_rows)
+
+    waits = []
+    tz = {}
+    rz = {}
+    for kz in (3, 2, 1):
+        g = flip(z, kz)
+        peer = dev(c, g, y, x)
+        tz[kz] = remote(tok_in.at[g], rows_out.at[me, :, xcols(x)],
+                        tz_send.at[kz], tz_recv.at[kz], peer)
+        tz[kz].start()
+        rz[kz] = remote(rw_in.at[g], rw_out.at[me], rz_send.at[kz], rz_recv.at[kz], peer)
+        rz[kz].start()
+    own_tok = pltpu.make_async_copy(tok_in.at[z], rows_out.at[me, :, xcols(x)], own.at[0])
+    own_tok.start()
+    own_rw = pltpu.make_async_copy(rw_in.at[z], rw_out.at[me], own.at[1])
+    own_rw.start()
+    ty = {}
+    tx = {}
+    ry = {}
+    ty[0] = remote(tok_in.at[z], rows_out.at[me, :, xcols(x)], ty_send.at[0], ty_recv.at[0], y_nbr)
+    ty[0].start()
+    ry[0] = remote(rw_in.at[z], rw_out.at[me], ry_send.at[0], ry_recv.at[0], y_nbr)
+    ry[0].start()
+    tx[0] = remote(tok_in.at[z], rows_out.at[me, :, xcols(x)], tx_send.at[0], tx_recv.at[0], x_nbr)
+    tx[0].start()
+
+    wsends = {}
+    for n, k in enumerate(ks):
+        pz, py = peer_of(k)
+        p = pz * n_y + py
+        if k != (0, 0):
+            for i, (src, dst) in enumerate(((gate_in, gate_out), (up_in, up_out))):
+                cp = remote(src.at[p], dst.at[0, grow(c, me)],
+                            w_send.at[3 * n + i], w_recv.at[3 * n + i], dev(c, pz, py, x))
+                cp.start()
+                wsends[n, i] = cp
+            cp = remote(down_in.at[p], down_out.at[0, drow(me), xcols(x)],
+                        w_send.at[3 * n + 2], w_recv.at[3 * n + 2], dev(x, pz, py, c))
+            cp.start()
+            wsends[n, 2] = cp
+        else:
+            own_w = []
+            for i, (src, dst) in enumerate(((gate_in, gate_out), (up_in, up_out))):
+                cp = pltpu.make_async_copy(src.at[me], dst.at[0, grow(c, me)], own.at[2 + i])
+                cp.start()
+                own_w.append(cp)
+                fw = remote(src.at[me], dst.at[0, grow(c, me)],
+                            f_send.at[3 * n + i], f_recv.at[3 * n + i], other)
+                fw.start()
+                waits.append(fw)
+            n_own = n
+            own_down = pltpu.make_async_copy(
+                down_in.at[me], down_out.at[0, drow(me), xcols(x)], own.at[4])
+            far_down = remote(down_in.at[me], down_out.at[0, drow(me), xcols(x)],
+                              w_send.at[3 * n + 2], w_recv.at[3 * n + 2], dev(x, z, y, c))
+
+            @pl.when(c == x)
+            def _():
+                own_down.start()
+
+            @pl.when(c != x)
+            def _():
+                far_down.start()
+
+    for kz in (1, 2, 3):
+        src = flip(z, kz) * n_y + y
+        tz[kz].wait_recv()
+        block = rows_out.at[src, :, xcols(x)]
+        ty[kz] = remote(block, block, ty_send.at[kz], ty_recv.at[kz], y_nbr)
+        ty[kz].start()
+        tx[kz] = remote(block, block, tx_send.at[kz], tx_recv.at[kz], x_nbr)
+        tx[kz].start()
+        rz[kz].wait_recv()
+        ry[kz] = remote(rw_out.at[src], rw_out.at[src], ry_send.at[kz], ry_recv.at[kz], y_nbr)
+        ry[kz].start()
+    for kz in (0, 1, 2, 3):
+        src = flip(z, kz) * n_y + 1 - y
+        ty[kz].wait_recv()
+        block = rows_out.at[src, :, xcols(x)]
+        tx[4 + kz] = remote(block, block, tx_send.at[4 + kz], tx_recv.at[4 + kz], x_nbr)
+        tx[4 + kz].start()
+
+    order = sorted(range(len(ks)), key=lambda n: (ks[n][0], ks[n][1]))
+    for n in order:
+        pz, py = peer_of(ks[n])
+        p = pz * n_y + py
+        if n != n_own:
+            for i, dst in enumerate((gate_out, up_out)):
+                wsends[n, i].wait_recv()
+                block = dst.at[0, grow(c, p)]
+                fw = remote(block, block, f_send.at[3 * n + i], f_recv.at[3 * n + i], other)
+                fw.start()
+                waits.append(fw)
+            wsends[n, 2].wait_recv()
+        else:
+
+            @pl.when(c == x)
+            def _():
+                own_down.wait()
+
+            @pl.when(c != x)
+            def _():
+                far_down.wait()
+
+        block = down_out.at[0, drow(p), xcols(c)]
+        fw = remote(block, block, f_send.at[3 * n + 2], f_recv.at[3 * n + 2], other)
+        fw.start()
+        waits.append(fw)
+
+    for cp in own_w + [own_tok, own_rw]:
+        cp.wait()
+    for cp in list(wsends.values()) + list(tz.values()) + list(rz.values()) + list(ty.values()):
+        cp.wait_send()
+    for cp in list(ry.values()) + list(tx.values()) + waits:
+        cp.wait()
+
+
+def hand_back(
+    n_z, n_y, p_in, ret_out,
+    rx1, ry1, s0, s1, ry2, rx2, fin,
+    a_send, a_recv, b_send, b_recv, z_send, z_recv, own,
+):
+    c, z, y, x = place(n_z, n_y)
+    dev = functools.partial(device, n_y=n_y)
+    x_nbr = dev(c, z, y, 1 - x)
+    y_nbr = dev(c, z, 1 - y, x)
+    greet([x_nbr, y_nbr] + [dev(c, flip(z, k), y, x) for k in (1, 2, 3)])
+    half = p_in.shape[3] // 2
+    q = half // 2
+
+    def cols(i, j):
+        return pl.ds(pl.multiple_of(i * half + j * q, q), q)
+
+    def add(a, b):
+        return (a.astype(jnp.float32) + b.astype(jnp.float32)).astype(BF16)
+
+    first = {}
+    for n, k in enumerate((3, 2, 1, 0)):
+        zs = flip(z, k)
+        moves = [
+            (p_in.at[0, zs, :, cols(1 - x, 0)], rx1.at[n, 0], x_nbr),
+            (p_in.at[1, zs, :, cols(1 - x, 0)], rx1.at[n, 1], x_nbr),
+            (p_in.at[1 - y, zs, :, cols(0, 1)], ry1.at[n, 0], y_nbr),
+            (p_in.at[1 - y, zs, :, cols(1, 1)], ry1.at[n, 1], y_nbr),
+        ]
+        for i, (src, dst, peer) in enumerate(moves):
+            first[n, i] = remote(src, dst, a_send.at[4 * n + i], a_recv.at[4 * n + i], peer)
+            first[n, i].start()
+    second = {}
+    for n, k in enumerate((3, 2, 1, 0)):
+        zs = flip(z, k)
+        for i in range(2):
+            first[n, i].wait_recv()
+            s0[n, i] = add(p_in[i, zs, :, cols(x, 0)], rx1[n, i])
+        second[n, 0] = remote(s0.at[n, 1 - y], ry2.at[n], b_send.at[2 * n], b_recv.at[2 * n], y_nbr)
+        second[n, 0].start()
+        for i in range(2):
+            first[n, 2 + i].wait_recv()
+            s1[n, i] = add(p_in[y, zs, :, cols(i, 1)], ry1[n, i])
+        second[n, 1] = remote(
+            s1.at[n, 1 - x], rx2.at[n], b_send.at[2 * n + 1], b_recv.at[2 * n + 1], x_nbr)
+        second[n, 1].start()
+    last = []
+    for n, k in enumerate((3, 2, 1, 0)):
+        second[n, 0].wait_recv()
+        fin[n, :, :q] = add(s0[n, y], ry2[n])
+        second[n, 1].wait_recv()
+        fin[n, :, q:] = add(s1[n, x], rx2[n])
+        if k:
+            cp = remote(fin.at[n], ret_out.at[z], z_send.at[n], z_recv.at[n],
+                        dev(c, flip(z, k), y, x))
+        else:
+            cp = pltpu.make_async_copy(fin.at[n], ret_out.at[z], own)
+        cp.start()
+        last.append(cp)
+    for cp in last:
+        cp.wait()
+    for cp in list(first.values()) + list(second.values()):
+        cp.wait_send()
+
+
+def paired(n_z, n_y, tokens, route_ids, route_weights, norm_gain, gate_weight, up_weight, down_weight):
+    gate_folded = (gate_weight * norm_gain[None, :, None]).astype(BF16)
+    up_folded = (up_weight * norm_gain[None, :, None]).astype(BF16)
+    down_rounded = down_weight.astype(BF16)
+    tok, width = tokens.shape
+    experts = gate_weight.shape[0]
+    epg = experts // GROUPS
+    cap = tok // GROUPS
+    half = width // lax.axis_size("tp")
+    x = lax.axis_index("tp")
+    n_fs = n_z * n_y
+
+    group = route_ids[:, 0] // epg
+    onehot = (group[:, None] == jnp.arange(GROUPS, dtype=jnp.int32)[None, :])
+    before = jnp.arange(tok)[:, None] >= jnp.arange(tok)[None, :]
+    upto = jnp.dot(before.astype(BF16), onehot.astype(BF16), preferred_element_type=jnp.float32)
+    slot = jnp.sum(jnp.where(onehot, upto, 0.0), axis=1).astype(jnp.int32) - 1
+    position = group * cap + slot
+    pick = position[None, :] == jnp.arange(tok, dtype=jnp.int32)[:, None]
+    pick_t = (position[:, None] == jnp.arange(tok, dtype=jnp.int32)[None, :]).astype(BF16)
+
+    widened = tokens.astype(jnp.float32)
+    scale = lax.rsqrt(jnp.mean(widened * widened, axis=-1, keepdims=True) + 1e-06)
+    mine = lax.dynamic_slice_in_dim(tokens, x * half, half, axis=1)
+    normed = (mine.astype(jnp.float32) * scale).astype(BF16)
+    outgoing = jnp.dot(pick.astype(BF16), normed, preferred_element_type=jnp.float32)
+    outgoing = outgoing.astype(BF16).reshape(GROUPS, cap, half)
+    even = route_ids[:, 0] % epg == 0
+    w_of = jnp.stack([
+        jnp.where(even, route_weights[:, 0], route_weights[:, 1]),
+        jnp.where(even, route_weights[:, 1], route_weights[:, 0]),
+    ])
+    w_sorted = jnp.sum(jnp.where(pick[None], w_of[:, None, :], 0.0), axis=2)
+    w_sorted = w_sorted.reshape(2, GROUPS, cap).transpose(1, 0, 2)
+    w_out = jnp.zeros((GROUPS, 8, -(-cap // 128) * 128), jnp.float32)
+    w_out = lax.dynamic_update_slice(w_out, w_sorted, (0, 0, 0))
+
+    hbm = pl.BlockSpec(memory_space=pl.ANY)
+    vmem = pl.BlockSpec(memory_space=pltpu.VMEM)
+    dma = pltpu.SemaphoreType.DMA
+    d_rows, d_cols = down_weight.shape[1:]
+    g_rows, g_cols = gate_weight.shape[1:]
+    gate_new, up_new, down_new, rows, w_in = pl.pallas_call(
+        functools.partial(hand_over, n_z, n_y),
+        out_shape=(
+            jax.ShapeDtypeStruct((1, 2 * n_fs * g_rows, g_cols), BF16),
+            jax.ShapeDtypeStruct((1, 2 * n_fs * g_rows, g_cols), BF16),
+            jax.ShapeDtypeStruct((1, n_fs * d_rows, 2 * d_cols), BF16),
+            jax.ShapeDtypeStruct((n_fs, cap, width), BF16),
+            jax.ShapeDtypeStruct((n_fs,) + w_out.shape[1:], jnp.float32),
+        ),
+        in_specs=[vmem] * 5,
+        out_specs=(hbm,) * 5,
+        scratch_shapes=[
+            dma((3 * n_fs,)), dma((3 * n_fs,)), dma((3 * n_fs,)), dma((3 * n_fs,)),
+            dma((4,)), dma((4,)), dma((4,)), dma((4,)), dma((8,)), dma((8,)),
+            dma((4,)), dma((4,)), dma((4,)), dma((4,)), dma((5,)), dma((1,)),
+        ],
+        compiler_params=pltpu.CompilerParams(collective_id=0, has_side_effects=True),
+    )(gate_folded, up_folded, down_rounded, outgoing, w_out)
+
+    y = lax.rem(lax.axis_index("fs"), n_y)
+    w_rows = lax.dynamic_index_in_dim(w_in, y, axis=1, keepdims=False)[:, :cap].reshape(n_fs * cap, 1)
+    flat = rows.reshape(n_fs * cap, width)
+    first = jnp.dot(flat, gate_new[0], preferred_element_type=jnp.float32)
+    second = jnp.dot(flat, up_new[0], preferred_element_type=jnp.float32)
+    hidden = (jax.nn.silu(first) * second).astype(BF16)
+    part = jnp.dot(hidden, down_new[0], preferred_element_type=jnp.float32) * w_rows
+    part = part.astype(BF16).reshape(n_z, n_y, cap, width).transpose(1, 0, 2, 3)
+
+    q = half // 2
+    ret = pl.pallas_call(
+        functools.partial(hand_back, n_z, n_y),
+        out_shape=jax.ShapeDtypeStruct((GROUPS, cap, half), BF16),
+        in_specs=[vmem],
+        out_specs=hbm,
+        scratch_shapes=[
+            pltpu.VMEM((4, 2, cap, q), BF16), pltpu.VMEM((4, 2, cap, q), BF16),
+            pltpu.VMEM((4, 2, cap, q), BF16), pltpu.VMEM((4, 2, cap, q), BF16),
+            pltpu.VMEM((4, cap, q), BF16), pltpu.VMEM((4, cap, q), BF16),
+            pltpu.VMEM((4, cap, half), BF16),
+            dma((16,)), dma((16,)), dma((8,)), dma((8,)), dma((4,)), dma((4,)), dma,
+        ],
+        compiler_params=pltpu.CompilerParams(collective_id=1, has_side_effects=True),
+    )(part)
+    mixed = jnp.dot(pick_t, ret.reshape(tok, half), preferred_element_type=jnp.float32)
+    return gate_new, up_new, down_new, mixed.astype(BF16)
+
+
 def solution(mesh):
     placed = (
         P(("gr", "fs"), None),
@@ -69,8 +409,16 @@
         P(None, ("gr", "fs"), "tp"),
         P(None, ("gr", "fs"), "tp"),
     )
+    n_fs = mesh.shape["fs"]
+
+    def body(*args):
+        experts = args[4].shape[0]
+        if experts == n_fs == 2 * GROUPS and mesh.shape["gr"] == mesh.shape["tp"] == 2:
+            return paired(GROUPS, 2, *args)
+        return local(*args)
+
     return jax.shard_map(
-        local,
+        body,
         mesh=mesh,
         in_specs=placed,
         out_specs=(

time: 331 us -> 185 us (0.56)
  waiting for transfers between devices: 193 us -> 0 us
  Pallas kernels: 0 us -> 149 us
  local copies, waits for them, and re-layouts: 50.7 us -> 9.46 us
  starting transfers between devices: 31.7 us -> 0 us
  other arithmetic: 27.2 us -> 7.74 us
  between operations: 14 us -> 0.71 us
  matrix products: 14 us -> 18.3 us
    all_to_all x6 -> x0, waiting for transfers between devices: 149 us -> none  [the longest x1 53.8 us: local(): lax.all_to_all(outgoing, 'fs', split_axis=0, concat_axis=0, tiled=True)]
    pallas_call x0 -> x2, Pallas kernels: none -> 149 us  [the longest x1 104 us: paired(): pl.pallas_call(functools.partial(hand_over, n_z, n_y), out_shape=(jax.Sha...]
    reduce_scatter x1 -> x0, waiting for transfers between devices: 41.7 us -> none  [local(): lax.psum_scatter(partial_out.reshape(senders, count, width).astype(jnp.bf...]
    all_to_all x6 -> x0, starting transfers between devices: 31.3 us -> none  [the longest x1 7.31 us: local(): lax.all_to_all(down_rounded, 'fs', split_axis=0, concat_axis=1, tiled=True)]
    unnamed x29 -> x17, local copies, waits for them, and re-layouts: 19.5 us -> 6.03 us
    unnamed x1 -> x0, other arithmetic: 12.8 us -> none
    gather x2 -> x0, local copies, waits for them, and re-layouts: 7.81 us -> none  [the longest x1 4.26 us: local(): outgoing = normed[source].reshape(experts, cap, width)]
    all_gather x1 -> x0, local copies, waits for them, and re-layouts: 6.77 us -> none  [local(): lax.all_gather(moved[2], 'gr', axis=1, tiled=True)]
  transfers between devices with their start and end apart: 10 -> 0, of which waited for: 6 -> 0; matrix products, arithmetic and copies ran while one was open for 19% -> 0% of each run, Pallas kernels for 0% -> 0%
where the time goes in v1:
time: 185 us
  Pallas kernels  149 us (81%)
  matrix products  18.3 us (10%)
  local copies, waits for them, and re-layouts  9.46 us (5%)
  other arithmetic  7.74 us (4%)
    pallas_call x1, Pallas kernels, paired(): pl.pallas_call(functools.partial(hand_over, n_z, n_y), out_shape=(jax.Sha...  104 us
    pallas_call x1, Pallas kernels, paired(): pl.pallas_call(functools.partial(hand_back, n_z, n_y), out_shape=jax.Shap...  44.3 us
    dot_general x1, matrix products, paired(): jnp.dot(hidden, down_new[0], preferred_element_type=jnp.float32) * w_rows  7.13 us
    unnamed x17, local copies, waits for them, and re-layouts  6.03 us
    dot_general x1, matrix products, paired(): first = jnp.dot(flat, gate_new[0], preferred_element_type=jnp.float32)  5.47 us

profile of v1, /device:TPU:0, one launch (start us, length us, event | category | flops | bytes accessed | tf_op | source)
XLA Modules:
  0.0 184.8 jit_solution(3192843177111083961)
XLA Ops:
  0.7 1.9 %multiply_reduce_fusion = f32[384]{0:T(512)S(1)} fusion(bf16[384,2048]{1,0:T(8,128)(2,1)} %param.7), kind=kLoop, calls=%fused_computation.2 | loop fusion | flops 2358912 | bytes 1574400 | tf_op jit(solution)/shard_map/reduce_sum | solution.py:335
  2.6 0.8 compare_select_fusion.6
  3.4 0.8 compare_select_fusion.5
  4.2 0.7 fusion.21
  4.9 0.2 fusion.7
  5.1 0.1 iota_compare_fusion.1
  5.2 0.3 select_reduce_fusion
  5.5 0.1 reshape.202
  5.6 0.6 dynamic_update_slice.3.rw_in
  6.2 2.8 %convolution_convert_fusion.1 = bf16[384,1024]{1,0:T(8,128)(2,1)} fusion(f32[384]{0:T(512)S(1)} %add_rsqrt_fusion, bf16[384,2048]{1,0:T(8,128)(2,1)} %param.7, s32[]{:T(128)S(6)} %select_n.70, s32[384]{0:T(512)S(1)} %get-tuple-element.20), kind=kOutput, calls=%fused_computation.13 | convolution fusion | flops 303710208 | bytes 1575940 | tf_op jit(solution)/shard_map/dot_general | solution.py:338
  9.0 1.1 convert_element_type.51.down_in
  10.2 2.0 %multiply_convert_fusion.1 = (bf16[8,128,512]{2,1,0:T(8,128)(2,1)}, bf16[8,128,512]{2,1,0:T(8,128)(2,1)}) fusion(f32[8,128,512]{2,1,0:T(8,128)S(1)} %copy-done, f32[128]{0:T(128)S(1)} %copy-done.6, f32[8,128,512]{2,1,0:T(8,128)S(1)} %copy-done.1), kind=kLoop, calls=%fused_computation.8 | loop fusion | flops 2097152 | bytes 6291968 | tf_op jit(solution)/shard_map/convert_element_type | solution.py:315
  12.2 104.3 %shard_map.102 = (bf16[1,2048,512]{2,1,0:T(8,128)(2,1)}, bf16[1,2048,512]{2,1,0:T(8,128)(2,1)}, bf16[1,512,2048]{2,1,0:T(8,128)(2,1)}, bf16[8,96,2048]{2,1,0:T(8,128)(2,1)}, f32[8,8,128]{2,1,0:T(8,128)}) custom-call(bf16[8,128,512]{2,1,0:T(8,128)(2,1)} %get-tuple-element.22.gate_in, bf16[8,128,512]{2,1,0:T(8,128)(2,1)} %get-tuple-element.21.up_in, ...), custom_call_target="tpu_custom_call" | custom-call | tf_op jit(solution)/shard_map/pallas_call | solution.py:355
  116.5 0.8 constant_dynamic-slice_fusion
  117.4 5.5 %fusion.3 = f32[768,512]{1,0:T(8,128)} fusion(bf16[768,2048]{1,0:T(8,128)(2,1)} %bitcast.43, bf16[1,2048,512]{2,1,0:T(8,128)(2,1)} %get-tuple-element.27), kind=kOutput, calls=%fused_computation.6 | convolution fusion | flops 1610612736 | bytes 6815744 | tf_op jit(solution)/shard_map/dot_general | solution.py:377
  122.8 7.1 %multiply_convert_fusion = bf16[768,2048]{1,0:T(8,128)(2,1)S(1)} fusion(f32[768]{0:T(1024)S(1)} %mul.73, bf16[1,512,2048]{2,1,0:T(8,128)(2,1)} %get-tuple-element.29, f32[768,512]{1,0:T(8,128)} %fusion.3, bf16[768,2048]{1,0:T(8,128)(2,1)} %bitcast.44, bf16[1,2048,512]{2,1,0:T(8,128)(2,1)} %get-tuple-element.28), kind=kOutput, calls=%fused_computation | convolution fusion | flops 3226730496 | bytes 12061696 | tf_op jit(solution)/shard_map/dot_general | solution.py:380
  130.0 1.9 %copy.17 = bf16[4,2,96,2048]{3,2,0,1:T(8,128)(2,1)} copy(bf16[4,2,96,2048]{3,2,1,0:T(8,128)(2,1)S(1)} %bitcast.38) | data formatting | bytes 6291456 | tf_op jit(solution)/shard_map/reshape | solution.py:381
  131.9 44.3 %shard_map.103 = bf16[4,96,1024]{2,1,0:T(8,128)(2,1)} custom-call(bf16[2,4,96,2048]{3,2,1,0:T(8,128)(2,1)} %bitcast.37), custom_call_target="tpu_custom_call" | custom-call | tf_op jit(solution)/shard_map/pallas_call | solution.py:384
  176.2 2.6 %convolution_convert_fusion = bf16[384,1024]{1,0:T(8,128)(2,1)} fusion(bf16[384,1024]{1,0:T(8,128)(2,1)} %bitcast.39, s32[384]{0:T(512)S(1)} %add_reduce_fusion), kind=kOutput, calls=%fused_computation.12 | convolution fusion | flops 302530560 | bytes 1574400 | tf_op jit(solution)/shard_map/dot_general | solution.py:398
  178.8 1.3 copy.22
  180.1 1.0 copy-done.4
  181.2 1.3 copy.23
  182.5 1.0 copy-done.3
  183.5 1.3 copy.24
  (18 shorter events, 0.2 us)
Async XLA Ops:
  0.6 8.4 %copy-start.2 = (f32[8,64,1024]{2,1,0:T(8,128)S(1)}, f32[8,64,1024]{2,1,0:T(8,128)}, u32[]{:S(2)}) copy-start(f32[8,64,1024]{2,1,0:T(8,128)} %param.13) | copy-start | bytes 6291460
  6.2 4.0 %copy-start = (f32[8,128,512]{2,1,0:T(8,128)S(1)}, f32[8,128,512]{2,1,0:T(8,128)}, u32[]{:S(2)}) copy-start(f32[8,128,512]{2,1,0:T(8,128)} %param.12) | copy-start | bytes 6291460
  6.2 4.0 %copy-start.1 = (f32[8,128,512]{2,1,0:T(8,128)S(1)}, f32[8,128,512]{2,1,0:T(8,128)}, u32[]{:S(2)}) copy-start(f32[8,128,512]{2,1,0:T(8,128)} %param.11) | copy-start | bytes 6291460
  6.2 4.0 %copy-start.6 = (f32[128]{0:T(128)S(1)}, f32[128]{0:T(128)}, u32[]{:S(2)}) copy-start(f32[128]{0:T(128)} %param.10) | copy-start | bytes 1540
  131.9 47.0 %copy-start.5 = (bf16[1,2048,512]{2,1,0:T(8,128)(2,1)S(1)}, bf16[1,2048,512]{2,1,0:T(8,128)(2,1)}, u32[]{:S(2)}) copy-start(bf16[1,2048,512]{2,1,0:T(8,128)(2,1)} %get-tuple-element.27) | copy-start | bytes 6291460
  178.8 2.3 %copy-start.4 = (bf16[1,2048,512]{2,1,0:T(8,128)(2,1)S(1)}, bf16[1,2048,512]{2,1,0:T(8,128)(2,1)}, u32[]{:S(2)}) copy-start(bf16[1,2048,512]{2,1,0:T(8,128)(2,1)} %get-tuple-element.28) | copy-start | bytes 6291460
  181.2 2.3 %copy-start.3 = (bf16[1,512,2048]{2,1,0:T(8,128)(2,1)S(1)}, bf16[1,512,2048]{2,1,0:T(8,128)(2,1)}, u32[]{:S(2)}) copy-start(bf16[1,512,2048]{2,1,0:T(8,128)(2,1)} %get-tuple-element.29) | copy-start | bytes 6291460

commit v2 on v0

--- a/solution.py
+++ b/solution.py
@@ -1,7 +1,16 @@
+import functools
+
 import jax
 import jax.numpy as jnp
 from jax import lax
+from jax.experimental import pallas as pl
+from jax.experimental.pallas import tpu as pltpu
 from jax.sharding import PartitionSpec as P
+
+GROUPS = 4
+HEAD = 2
+BF16 = jnp.bfloat16
+MESH = pl.DeviceIdType.MESH
 
 
 def local(tokens, route_ids, route_weights, norm_gain, gate_weight, up_weight, down_weight):
@@ -59,6 +68,361 @@
     return (gate_new, up_new, down_new, mixed)
 
 
+def place(n_z, n_y):
+    f = lax.axis_index("fs")
+    return lax.axis_index("gr"), f // n_y, lax.rem(f, n_y), lax.axis_index("tp")
+
+
+def flip(z, k):
+    return (z, z + 1 - 2 * lax.rem(z, 2), lax.rem(z + 2, 4), 3 - z)[k]
+
+
+def device(c, z, y, x, n_y):
+    return {"gr": c, "fs": z * n_y + y, "tp": x}
+
+
+def greet(peers):
+    barrier = pltpu.get_barrier_semaphore()
+    for peer in peers:
+        pl.semaphore_signal(barrier, inc=1, device_id=peer, device_id_type=MESH)
+    pl.semaphore_wait(barrier, len(peers))
+
+
+def remote(src, dst, send, recv, peer):
+    return pltpu.make_async_remote_copy(
+        src_ref=src, dst_ref=dst, send_sem=send, recv_sem=recv,
+        device_id=peer, device_id_type=MESH,
+    )
+
+
+def sampler(
+    n_z, n_y,
+    tok_in, group_in, rw_in, gain_in, gate_in, up_in, down_in,
+    gate_out, up_out, down_out, mixed_out,
+    wide, narrow, dwide, dnarrow, land, dland, dcross,
+    normed, tok_s, rows, rw_s, rw_l, hid, out_s, ry_l, fin, ret,
+    ld_sem, w_send, w_recv, f_send, f_recv,
+    tz_send, tz_recv, ty_send, ty_recv, tx_send, tx_recv,
+    rz_send, rz_recv, ry_send, ry_recv,
+    h_send, h_recv, c_send, c_recv, y_send, y_recv, z_send, z_recv, o_sem,
+):
+    c, z, y, x = place(n_z, n_y)
+    me = z * n_y + y
+    n_fs = n_z * n_y
+    g_rows, d_rows = gate_in.shape[1], down_in.shape[1]
+    tok, width = tok_in.shape
+    half = width // 2
+    cap = tok // GROUPS
+    hb = hid.shape[2]
+    f32 = jnp.float32
+    dev = functools.partial(device, n_y=n_y)
+    ks = [(kz, ky) for kz in (3, 2, 1, 0) for ky in (1, 0)]
+    last = len(ks) - 1
+    at = []
+    for kz, ky in ks:
+        pz, py = flip(z, kz), (1 - y if ky else y)
+        at.append((pz * n_y + py, dev(c, pz, py, x)))
+    other = dev(1 - c, z, y, x)
+    x_nbr = dev(c, z, y, 1 - x)
+    y_nbr = dev(c, z, 1 - y, x)
+
+    def xcols(i):
+        return pl.ds(pl.multiple_of(i * half, half), half)
+
+    def grow(core, f):
+        return pl.ds(pl.multiple_of((core * n_fs + f) * g_rows, g_rows), g_rows)
+
+    def drow(core, f):
+        return pl.ds(pl.multiple_of((core * n_fs + f) * d_rows, d_rows), d_rows)
+
+    def trow(f):
+        return pl.ds(pl.multiple_of(f * cap, cap), cap)
+
+    pair = (gate_in, up_in)
+    loads = {}
+    for n, (p, _) in enumerate(at):
+        for i in range(2):
+            loads[n, i] = pltpu.make_async_copy(pair[i].at[p], wide.at[i, n], ld_sem.at[3 * n + i])
+            loads[n, i].start()
+    for n, (p, _) in enumerate(at):
+        loads[n, 2] = pltpu.make_async_copy(down_in.at[p], dwide.at[n], ld_sem.at[3 * n + 2])
+        loads[n, 2].start()
+    greet([d for _, d in at[:last]] + [other, x_nbr])
+
+    def column(row, count):
+        lanes = row.shape[1]
+        eye = (lax.broadcasted_iota(jnp.int32, (count, lanes), 0)
+               == lax.broadcasted_iota(jnp.int32, (count, lanes), 1))
+        return jnp.sum(jnp.where(eye, row, 0.0), axis=1, keepdims=True)
+
+    gain = column(gain_in[...], g_rows)
+    sends = []
+    arrive = {}
+    onward = {}
+
+    def fold(n):
+        p, peer = at[n]
+        for i in range(2):
+            loads[n, i].wait()
+            value = (wide[i, n] * gain).astype(BF16)
+            if n == last:
+                land[i, grow(c, me)] = value
+                block = land.at[i, grow(c, me)]
+                onward[n, i] = remote(block, block, f_send.at[3 * n + i], f_recv.at[3 * n + i], other)
+                onward[n, i].start()
+            else:
+                narrow[i, n] = value
+                cp = remote(narrow.at[i, n], land.at[i, grow(c, me)],
+                            w_send.at[3 * n + i], w_recv.at[3 * n + i], peer)
+                cp.start()
+                arrive[n, i] = cp
+
+    for n in range(HEAD):
+        fold(n)
+
+    def norm_rows(i, carry):
+        r = pl.ds(pl.multiple_of(i * cap, cap), cap)
+        v = tok_in[r, :].astype(f32)
+        scale = lax.rsqrt(jnp.mean(v * v, axis=-1, keepdims=True) + 1e-06)
+        normed[r, :] = (tok_in[r, xcols(x)].astype(f32) * scale).astype(BF16)
+        return carry
+
+    lax.fori_loop(0, GROUPS, norm_rows, 0)
+    group = group_in[...]
+    onehot = (lax.broadcasted_iota(jnp.int32, (8, tok), 0) == group).astype(f32)
+    upto = (lax.broadcasted_iota(jnp.int32, (tok, tok), 0)
+            <= lax.broadcasted_iota(jnp.int32, (tok, tok), 1)).astype(BF16)
+    count = jnp.dot(onehot.astype(BF16), upto, preferred_element_type=f32)
+    slot = jnp.sum(onehot * count, axis=0, keepdims=True).astype(jnp.int32) - 1
+    position = group * cap + slot
+
+    def picked(g):
+        return lax.broadcasted_iota(jnp.int32, (cap, tok), 0) + g * cap == position
+
+    tz, rz, ty, tx, ry = {}, {}, {}, {}, {}
+    for kz in (3, 2, 1, 0):
+        g = flip(z, kz)
+        pick = picked(g)
+        block = jnp.dot(pick.astype(BF16), normed[...], preferred_element_type=f32).astype(BF16)
+        w_row = lax.dot_general(rw_in[...], pick.astype(f32), (((1,), (1,)), ((), ())),
+                                precision=lax.Precision.HIGHEST, preferred_element_type=f32)
+        if kz:
+            tok_s[kz] = block
+            rw_s[kz, :, :cap] = w_row
+            peer = dev(c, g, y, x)
+            tz[kz] = remote(tok_s.at[kz], rows.at[trow(me), xcols(x)],
+                            tz_send.at[kz], tz_recv.at[kz], peer)
+            tz[kz].start()
+            rz[kz] = remote(rw_s.at[kz], rw_l.at[me], rz_send.at[kz], rz_recv.at[kz], peer)
+            rz[kz].start()
+        else:
+            rows[trow(me), xcols(x)] = block
+            rw_l[me, :, :cap] = w_row
+
+    def pass_on(kz):
+        src = flip(z, kz) * n_y + y
+        block = rows.at[trow(src), xcols(x)]
+        ty[kz] = remote(block, block, ty_send.at[kz], ty_recv.at[kz], y_nbr)
+        ty[kz].start()
+        tx[kz] = remote(block, block, tx_send.at[kz], tx_recv.at[kz], x_nbr)
+        tx[kz].start()
+        ry[kz] = remote(rw_l.at[src], rw_l.at[src], ry_send.at[kz], ry_recv.at[kz], y_nbr)
+        ry[kz].start()
+
+    pass_on(0)
+    for n in range(HEAD, len(ks)):
+        fold(n)
+    for n, (p, peer) in enumerate(at):
+        loads[n, 2].wait()
+        value = dwide[n].astype(BF16)
+        if n == last:
+            dland[drow(c, me)] = value
+            block = dland.at[drow(c, me)]
+            onward[n, 2] = remote(block, block, f_send.at[3 * n + 2], f_recv.at[3 * n + 2], other)
+            onward[n, 2].start()
+        else:
+            dnarrow[n] = value
+            arrive[n, 2] = remote(dnarrow.at[n], dland.at[drow(c, me)],
+                                  w_send.at[3 * n + 2], w_recv.at[3 * n + 2], peer)
+            arrive[n, 2].start()
+
+    for kz in (1, 2, 3):
+        tz[kz].wait_recv()
+        rz[kz].wait_recv()
+        pass_on(kz)
+    for kz in (0, 1, 2, 3):
+        ty[kz].wait_recv()
+        block = rows.at[trow(flip(z, kz) * n_y + 1 - y), xcols(x)]
+        tx[4 + kz] = remote(block, block, tx_send.at[4 + kz], tx_recv.at[4 + kz], x_nbr)
+        tx[4 + kz].start()
+
+    order = sorted(range(last), key=lambda n: ks[n])
+    for n in order:
+        for i in range(2):
+            arrive[n, i].wait_recv()
+            block = land.at[i, grow(c, at[n][0])]
+            onward[n, i] = remote(block, block, f_send.at[3 * n + i], f_recv.at[3 * n + i], other)
+            onward[n, i].start()
+    for cp in list(tx.values()) + list(ry.values()):
+        cp.wait_recv()
+    for n in [last] + order:
+        for i in range(2):
+            onward[n, i].wait_recv()
+    outs = []
+    for i, out in enumerate((gate_out, up_out)):
+        cp = pltpu.make_async_copy(land.at[i], out.at[0], o_sem.at[i])
+        cp.start()
+        outs.append(cp)
+
+    m, q = rows.shape[0] // 2, 256
+    hsend = []
+    for j in range(2):
+        r = pl.ds(j * m, m)
+
+        def units(i, carry):
+            s = pl.ds(pl.multiple_of(i * q, q), q)
+            a = jnp.dot(rows[r, :], land[0, :, s], preferred_element_type=f32)
+            b = jnp.dot(rows[r, :], land[1, :, s], preferred_element_type=f32)
+            hid[x, r, s] = (a / (1.0 + jnp.exp(-a)) * b).astype(BF16)
+            return carry
+
+        lax.fori_loop(0, hb // q, units, 0)
+        cp = remote(hid.at[x, r], hid.at[x, r], h_send.at[j], h_recv.at[j], x_nbr)
+        cp.start()
+        hsend.append(cp)
+
+    for n in order:
+        arrive[n, 2].wait_recv()
+        block = dland.at[drow(c, at[n][0])]
+        onward[n, 2] = remote(block, block, f_send.at[3 * n + 2], f_recv.at[3 * n + 2], other)
+        onward[n, 2].start()
+    for n in [last] + order:
+        onward[n, 2].wait_recv()
+    for cp in hsend:
+        cp.wait_recv()
+    part = hb // 2
+    mine = pl.ds(pl.multiple_of(c * part, part), part)
+    cross = remote(
+        dland.at[pl.ds(pl.multiple_of((1 - x) * hb + c * part, part), part)],
+        dcross.at[mine], c_send.at[0], c_recv.at[0], x_nbr)
+    cross.start()
+    cp = pltpu.make_async_copy(
+        dland.at[pl.ds(pl.multiple_of(x * hb, hb), hb)], down_out.at[0, :, xcols(x)], o_sem.at[2])
+    cp.start()
+    outs.append(cp)
+
+    ysend = []
+    for n, kz in enumerate((3, 2, 1, 0)):
+        zs = flip(z, kz)
+        for step in range(2):
+            s = 1 - y if step == 0 else y
+            f = zs * n_y + s
+            acc = jnp.dot(hid[0, trow(f)], dland[:hb], preferred_element_type=f32)
+            acc += jnp.dot(hid[1, trow(f)], dland[hb:], preferred_element_type=f32)
+            w = jnp.where(y == 0, rw_l[f, 0:1, :], rw_l[f, 1:2, :])
+            lane = lax.broadcasted_iota(jnp.int32, w.shape, 1)
+            w = jnp.where(lane < cap, w, 0.0)
+            out_s[n, step] = (acc * column(w, cap)).astype(BF16)
+            if step == 0:
+                cp = remote(out_s.at[n, 0], ry_l.at[n], y_send.at[n], y_recv.at[n], y_nbr)
+                cp.start()
+                ysend.append(cp)
+    zsend = []
+    for n, kz in enumerate((3, 2, 1, 0)):
+        ysend[n].wait_recv()
+        total = (out_s[n, 1].astype(f32) + ry_l[n].astype(f32)).astype(BF16)
+        if kz:
+            fin[n] = total
+            cp = remote(fin.at[n], ret.at[trow(z)], z_send.at[n], z_recv.at[n],
+                        dev(c, flip(z, kz), y, x))
+            cp.start()
+            zsend.append(cp)
+        else:
+            ret[trow(z)] = total
+
+    cross.wait_recv()
+    over = remote(dcross.at[mine], dcross.at[mine], c_send.at[1], c_recv.at[1], other)
+    over.start()
+    for cp in zsend:
+        cp.wait_recv()
+    everyone = (lax.broadcasted_iota(jnp.int32, (tok, tok), 0) == position).astype(BF16)
+    mixed_out[...] = lax.dot_general(
+        everyone, ret[...], (((0,), (0,)), ((), ())), preferred_element_type=f32).astype(BF16)
+    over.wait_recv()
+    cp = pltpu.make_async_copy(dcross, down_out.at[0, :, xcols(1 - x)], o_sem.at[3])
+    cp.start()
+    outs.append(cp)
+    for cp in outs:
+        cp.wait()
+    for group_of in (arrive, onward, tz, rz, ty, tx, ry):
+        for cp in group_of.values():
+            cp.wait_send()
+    for cp in hsend + ysend + zsend + [cross, over]:
+        cp.wait_send()
+
+
+def paired(n_z, n_y, tokens, route_ids, route_weights, norm_gain, gate_weight, up_weight, down_weight):
+    tok, width = tokens.shape
+    experts = gate_weight.shape[0]
+    epg = experts // GROUPS
+    cap = tok // GROUPS
+    half = width // lax.axis_size("tp")
+    n_fs = n_z * n_y
+    d_rows, d_cols = down_weight.shape[1:]
+    g_rows, g_cols = gate_weight.shape[1:]
+    f32 = jnp.float32
+
+    group = (route_ids[:, 0] // epg).reshape(1, tok)
+    even = route_ids[:, 0] % epg == 0
+    w_first, w_second = route_weights[:, 0], route_weights[:, 1]
+    w_of = jnp.stack([jnp.where(even, w_first, w_second), jnp.where(even, w_second, w_first)])
+    w_of = jnp.pad(w_of, ((0, 6), (0, 0)))
+
+    hbm = pl.BlockSpec(memory_space=pl.ANY)
+    vmem = pl.BlockSpec(memory_space=pltpu.VMEM)
+    dma = pltpu.SemaphoreType.DMA
+    lanes = -(-cap // 128) * 128
+    gate_new, up_new, down_new, mixed = pl.pallas_call(
+        functools.partial(sampler, n_z, n_y),
+        out_shape=(
+            jax.ShapeDtypeStruct((1, 2 * n_fs * g_rows, g_cols), BF16),
+            jax.ShapeDtypeStruct((1, 2 * n_fs * g_rows, g_cols), BF16),
+            jax.ShapeDtypeStruct((1, n_fs * d_rows, 2 * d_cols), BF16),
+            jax.ShapeDtypeStruct((tok, half), BF16),
+        ),
+        in_specs=[vmem] * 4 + [hbm] * 3,
+        out_specs=(hbm, hbm, hbm, vmem),
+        scratch_shapes=[
+            pltpu.VMEM((2, n_fs, g_rows, g_cols), f32),
+            pltpu.VMEM((2, n_fs - 1, g_rows, g_cols), BF16),
+            pltpu.VMEM((n_fs, d_rows, d_cols), f32),
+            pltpu.VMEM((n_fs - 1, d_rows, d_cols), BF16),
+            pltpu.VMEM((2, 2 * n_fs * g_rows, g_cols), BF16),
+            pltpu.VMEM((2 * n_fs * d_rows, d_cols), BF16),
+            pltpu.VMEM((n_fs * d_rows, d_cols), BF16),
+            pltpu.VMEM((tok, half), BF16),
+            pltpu.VMEM((4, cap, half), BF16),
+            pltpu.VMEM((n_fs * cap, width), BF16),
+            pltpu.VMEM((4, 8, lanes), f32),
+            pltpu.VMEM((n_fs, 8, lanes), f32),
+            pltpu.VMEM((2, n_fs * cap, n_fs * d_rows), BF16),
+            pltpu.VMEM((4, 2, cap, half), BF16),
+            pltpu.VMEM((4, cap, half), BF16),
+            pltpu.VMEM((4, cap, half), BF16),
+            pltpu.VMEM((GROUPS * cap, half), BF16),
+            dma((3 * n_fs,)),
+            dma((3 * n_fs,)), dma((3 * n_fs,)), dma((3 * n_fs,)), dma((3 * n_fs,)),
+            dma((4,)), dma((4,)), dma((4,)), dma((4,)), dma((8,)), dma((8,)),
+            dma((4,)), dma((4,)), dma((4,)), dma((4,)),
+            dma((2,)), dma((2,)), dma((2,)), dma((2,)), dma((4,)), dma((4,)),
+            dma((4,)), dma((4,)), dma((4,)),
+        ],
+        compiler_params=pltpu.CompilerParams(
+            collective_id=0, has_side_effects=True, vmem_limit_bytes=56 * 1024 * 1024),
+    )(tokens, group, w_of, norm_gain.reshape(1, g_rows), gate_weight, up_weight, down_weight)
+    return gate_new, up_new, down_new, mixed
+
+
 def solution(mesh):
     placed = (
         P(("gr", "fs"), None),
@@ -69,8 +433,16 @@
         P(None, ("gr", "fs"), "tp"),
         P(None, ("gr", "fs"), "tp"),
     )
+    n_fs = mesh.shape["fs"]
+
+    def body(*args):
+        experts = args[4].shape[0]
+        if experts == n_fs == 2 * GROUPS and mesh.shape["gr"] == mesh.shape["tp"] == 2:
+            return paired(GROUPS, 2, *args)
+        return local(*args)
+
     return jax.shard_map(
-        local,
+        body,
         mesh=mesh,
         in_specs=placed,
         out_specs=(

time: 331 us -> 153 us (0.46)
  the two profiles are of different devices: /device:TPU:0 before, /device:TPU:12 now
where the time goes in v2:
time: 153 us; the launch traced here: 152 us
  Pallas kernels  140 us (92%)
  local copies, waits for them, and re-layouts  8.1 us (5%)
  other arithmetic  3.4 us (2%)
    pallas_call x1, Pallas kernels, paired(): pl.pallas_call(functools.partial(sampler, n_z, n_y), out_shape=(jax.Shape...  140 us
    unnamed x10, local copies, waits for them, and re-layouts  8.1 us

profile of v2, /device:TPU:12, one launch (start us, length us, event | category | flops | bytes accessed | tf_op | source)
XLA Modules:
  0.0 152.4 jit_solution(9385811164524120855)
XLA Ops:
  0.6 0.8 compare_select_fusion.4
  1.4 0.8 compare_select_fusion.3
  2.2 1.3 and_select_fusion.1.group_in
  3.4 0.6 select_maximum_fusion.rw_in
  4.0 140.2 %shard_map.102 = (bf16[1,2048,512]{2,1,0:T(8,128)(2,1)}, bf16[1,2048,512]{2,1,0:T(8,128)(2,1)}, bf16[1,512,2048]{2,1,0:T(8,128)(2,1)}, bf16[384,1024]{1,0:T(8,128)(2,1)}) custom-call(bf16[384,2048]{1,0:T(8,128)(2,1)} %tok_in.1, s32[1,384]{1,0:T(1,128)} %and_select_fusion.1.group_in, f32[8,384]{1,0:T(8,128)} %select_maximum_fusion.rw_in, f32[1,128]{1,0:T(1,128)} %bitcast.19, ...), custom_call_target="tpu_custom_call" | custom-call | tf_op jit(solution)/shard_map/pallas_call | solution.py:385
  144.2 0.0 copy-start.1
  144.3 3.2 %copy.15 = bf16[1,2048,512]{2,1,0:T(8,128)(2,1)} copy(bf16[1,2048,512]{2,1,0:T(8,128)(2,1)} %get-tuple-element.10) | data formatting | bytes 4194304
  147.4 0.0 copy-done.1
  147.4 0.0 copy-start
  147.4 1.3 copy.16
  148.8 1.0 copy-done
  149.8 0.0 copy-start.2
  149.8 1.3 copy.17
  151.1 0.4 copy-done.2
  151.5 0.9 copy.18
Async XLA Ops:
  144.2 3.2 %copy-start.1 = (bf16[1,2048,512]{2,1,0:T(8,128)(2,1)S(1)}, bf16[1,2048,512]{2,1,0:T(8,128)(2,1)}, u32[]{:S(2)}) copy-start(bf16[1,2048,512]{2,1,0:T(8,128)(2,1)} %get-tuple-element.11) | copy-start | bytes 6291460
  147.4 2.3 %copy-start = (bf16[1,512,2048]{2,1,0:T(8,128)(2,1)S(1)}, bf16[1,512,2048]{2,1,0:T(8,128)(2,1)}, u32[]{:S(2)}) copy-start(bf16[1,512,2048]{2,1,0:T(8,128)(2,1)} %get-tuple-element.12) | copy-start | bytes 6291460
  149.8 1.7 %copy-start.2 = (bf16[384,1024]{1,0:T(8,128)(2,1)S(1)}, bf16[384,1024]{1,0:T(8,128)(2,1)}, u32[]{:S(2)}) copy-start(bf16[384,1024]{1,0:T(8,128)(2,1)} %get-tuple-element.13) | copy-start | bytes 2359300

commit v3 on v2

--- a/solution.py
+++ b/solution.py
@@ -97,7 +97,7 @@
 
 def sampler(
     n_z, n_y,
-    tok_in, group_in, rw_in, gain_in, gate_in, up_in, down_in,
+    tok_in, ids_in, rw_in, gain_in, gate_in, up_in, down_in,
     gate_out, up_out, down_out, mixed_out,
     wide, narrow, dwide, dnarrow, land, dland, dcross,
     normed, tok_s, rows, rw_s, rw_l, hid, out_s, ry_l, fin, ret,
@@ -116,7 +116,7 @@
     hb = hid.shape[2]
     f32 = jnp.float32
     dev = functools.partial(device, n_y=n_y)
-    ks = [(kz, ky) for kz in (3, 2, 1, 0) for ky in (1, 0)]
+    ks = [(kz, ky) for kz in (1, 3, 2, 0) for ky in (1, 0)]
     last = len(ks) - 1
     at = []
     for kz, ky in ks:
@@ -156,7 +156,6 @@
         return jnp.sum(jnp.where(eye, row, 0.0), axis=1, keepdims=True)
 
     gain = column(gain_in[...], g_rows)
-    sends = []
     arrive = {}
     onward = {}
 
@@ -188,7 +187,16 @@
         return carry
 
     lax.fori_loop(0, GROUPS, norm_rows, 0)
-    group = group_in[...]
+    epg = gate_in.shape[0] // GROUPS
+    low = ids_in[0:1, :]
+    group = jnp.zeros_like(low)
+    for g in range(1, GROUPS):
+        group += (low >= g * epg).astype(jnp.int32)
+    ahead = low == group * epg
+    w_a, w_b = rw_in[0:1, :], rw_in[1:2, :]
+    sub = lax.broadcasted_iota(jnp.int32, (8, tok), 0)
+    w_of = jnp.where(sub == 0, jnp.where(ahead, w_a, w_b),
+                     jnp.where(sub == 1, jnp.where(ahead, w_b, w_a), 0.0))
     onehot = (lax.broadcasted_iota(jnp.int32, (8, tok), 0) == group).astype(f32)
     upto = (lax.broadcasted_iota(jnp.int32, (tok, tok), 0)
             <= lax.broadcasted_iota(jnp.int32, (tok, tok), 1)).astype(BF16)
@@ -200,11 +208,11 @@
         return lax.broadcasted_iota(jnp.int32, (cap, tok), 0) + g * cap == position
 
     tz, rz, ty, tx, ry = {}, {}, {}, {}, {}
-    for kz in (3, 2, 1, 0):
+    for kz in (1, 3, 2, 0):
         g = flip(z, kz)
         pick = picked(g)
         block = jnp.dot(pick.astype(BF16), normed[...], preferred_element_type=f32).astype(BF16)
-        w_row = lax.dot_general(rw_in[...], pick.astype(f32), (((1,), (1,)), ((), ())),
+        w_row = lax.dot_general(w_of, pick.astype(f32), (((1,), (1,)), ((), ())),
                                 precision=lax.Precision.HIGHEST, preferred_element_type=f32)
         if kz:
             tok_s[kz] = block
@@ -312,7 +320,7 @@
     outs.append(cp)
 
     ysend = []
-    for n, kz in enumerate((3, 2, 1, 0)):
+    for n, kz in enumerate((3, 1, 2, 0)):
         zs = flip(z, kz)
         for step in range(2):
             s = 1 - y if step == 0 else y
@@ -328,7 +336,7 @@
                 cp.start()
                 ysend.append(cp)
     zsend = []
-    for n, kz in enumerate((3, 2, 1, 0)):
+    for n, kz in enumerate((3, 1, 2, 0)):
         ysend[n].wait_recv()
         total = (out_s[n, 1].astype(f32) + ry_l[n].astype(f32)).astype(BF16)
         if kz:
@@ -363,20 +371,12 @@
 
 def paired(n_z, n_y, tokens, route_ids, route_weights, norm_gain, gate_weight, up_weight, down_weight):
     tok, width = tokens.shape
-    experts = gate_weight.shape[0]
-    epg = experts // GROUPS
     cap = tok // GROUPS
     half = width // lax.axis_size("tp")
     n_fs = n_z * n_y
     d_rows, d_cols = down_weight.shape[1:]
     g_rows, g_cols = gate_weight.shape[1:]
     f32 = jnp.float32
-
-    group = (route_ids[:, 0] // epg).reshape(1, tok)
-    even = route_ids[:, 0] % epg == 0
-    w_first, w_second = route_weights[:, 0], route_weights[:, 1]
-    w_of = jnp.stack([jnp.where(even, w_first, w_second), jnp.where(even, w_second, w_first)])
-    w_of = jnp.pad(w_of, ((0, 6), (0, 0)))
 
     hbm = pl.BlockSpec(memory_space=pl.ANY)
     vmem = pl.BlockSpec(memory_space=pltpu.VMEM)
@@ -390,7 +390,7 @@
             jax.ShapeDtypeStruct((1, n_fs * d_rows, 2 * d_cols), BF16),
             jax.ShapeDtypeStruct((tok, half), BF16),
         ),
-        in_specs=[vmem] * 4 + [hbm] * 3,
+        in_specs=[vmem] * 4 + [pl.BlockSpec(memory_space=pltpu.HBM)] * 3,
         out_specs=(hbm, hbm, hbm, vmem),
         scratch_shapes=[
             pltpu.VMEM((2, n_fs, g_rows, g_cols), f32),
@@ -418,8 +418,8 @@
             dma((4,)), dma((4,)), dma((4,)),
         ],
         compiler_params=pltpu.CompilerParams(
-            collective_id=0, has_side_effects=True, vmem_limit_bytes=56 * 1024 * 1024),
-    )(tokens, group, w_of, norm_gain.reshape(1, g_rows), gate_weight, up_weight, down_weight)
+            collective_id=0, has_side_effects=True, vmem_limit_bytes=36 * 1024 * 1024),
+    )(tokens, route_ids.T, route_weights.T, norm_gain.reshape(1, g_rows), gate_weight, up_weight, down_weight)
     return gate_new, up_new, down_new, mixed
 
 

time: 153 us -> 142 us (0.928)
  the two profiles are of different devices: /device:TPU:12 before, /device:TPU:0 now
where the time goes in v3:
time: 142 us; the launch traced here: 141 us
  Pallas kernels  128 us (90%)
  local copies, waits for them, and re-layouts  13 us (9%)
    pallas_call x1, Pallas kernels, paired(): pl.pallas_call(functools.partial(sampler, n_z, n_y), out_shape=(jax.Shape...  128 us
    unnamed x18, local copies, waits for them, and re-layouts  13 us

profile of v3, /device:TPU:0, one launch (start us, length us, event | category | flops | bytes accessed | tf_op | source)
XLA Modules:
  0.0 141.4 jit_solution(13991156795976114034)
XLA Ops:
  0.6 0.0 copy-start
  0.6 1.6 %copy-done = f32[8,128,512]{2,1,0:T(8,128)S(1)} copy-done((f32[8,128,512]{2,1,0:T(8,128)S(1)}, f32[8,128,512]{2,1,0:T(8,128)}, u32[]{:S(2)}) %copy-start) | copy-done | bytes 2097176
  2.2 0.0 copy-start.1
  2.2 1.6 %copy-done.1 = f32[8,128,512]{2,1,0:T(8,128)S(1)} copy-done((f32[8,128,512]{2,1,0:T(8,128)S(1)}, f32[8,128,512]{2,1,0:T(8,128)}, u32[]{:S(2)}) %copy-start.1) | copy-done | bytes 2097176
  3.8 0.0 copy-start.2
  3.8 1.6 %copy-done.2 = f32[8,64,1024]{2,1,0:T(8,128)S(1)} copy-done((f32[8,64,1024]{2,1,0:T(8,128)S(1)}, f32[8,64,1024]{2,1,0:T(8,128)}, u32[]{:S(2)}) %copy-start.2) | copy-done | bytes 2097176
  5.4 0.0 copy-start.3
  5.4 1.4 copy-done.3
  6.8 0.0 copy-start.4
  6.8 0.7 copy-done.4
  7.5 0.0 copy-start.5
  7.5 0.7 copy-done.5
  8.2 0.0 copy-start.6
  8.2 0.7 copy-done.6
  8.8 127.7 %shard_map.102 = (bf16[1,2048,512]{2,1,0:T(8,128)(2,1)S(1)}, bf16[1,2048,512]{2,1,0:T(8,128)(2,1)S(1)}, bf16[1,512,2048]{2,1,0:T(8,128)(2,1)S(1)}, bf16[384,1024]{1,0:T(8,128)(2,1)S(1)}) custom-call(bf16[384,2048]{1,0:T(8,128)(2,1)S(1)} %copy-done.3, s32[2,384]{1,0:T(2,128)S(1)} %bitcast.3, f32[2,384]{1,0:T(2,128)S(1)} %bitcast.4, f32[1,128]{1,0:T(1,128)S(1)} %bitcast.5, ...), custom_call_target="tpu_custom_call" | custom-call | tf_op jit(solution)/shard_map/pallas_call | solution.py:385
  136.6 1.3 copy.15
  137.9 1.3 copy.16
  139.2 1.3 copy.17
  140.5 0.9 copy.18
Async XLA Ops:
  0.6 1.6 %copy-start = (f32[8,128,512]{2,1,0:T(8,128)S(1)}, f32[8,128,512]{2,1,0:T(8,128)}, u32[]{:S(2)}) copy-start(f32[8,128,512]{2,1,0:T(8,128)} %gate_in.1) | copy-start | bytes 6291460
  2.2 1.6 %copy-start.1 = (f32[8,128,512]{2,1,0:T(8,128)S(1)}, f32[8,128,512]{2,1,0:T(8,128)}, u32[]{:S(2)}) copy-start(f32[8,128,512]{2,1,0:T(8,128)} %up_in.1) | copy-start | bytes 6291460
  3.8 1.6 %copy-start.2 = (f32[8,64,1024]{2,1,0:T(8,128)S(1)}, f32[8,64,1024]{2,1,0:T(8,128)}, u32[]{:S(2)}) copy-start(f32[8,64,1024]{2,1,0:T(8,128)} %down_in.1) | copy-start | bytes 6291460
  5.4 1.4 copy-start.3
  6.8 0.7 copy-start.4
  7.5 0.7 copy-start.5
  8.2 0.7 copy-start.6

commit v4 on v3

--- a/solution.py
+++ b/solution.py
@@ -9,6 +9,9 @@
 
 GROUPS = 4
 HEAD = 2
+MID = 3
+PIECES = 2
+RETURN = (3, 1, 2, 0)
 BF16 = jnp.bfloat16
 MESH = pl.DeviceIdType.MESH
 
@@ -116,7 +119,7 @@
     hb = hid.shape[2]
     f32 = jnp.float32
     dev = functools.partial(device, n_y=n_y)
-    ks = [(kz, ky) for kz in (1, 3, 2, 0) for ky in (1, 0)]
+    ks = [(kz, 0) for kz in (1, 3, 2)] + [(kz, 1) for kz in (1, 3, 2, 0)] + [(0, 0)]
     last = len(ks) - 1
     at = []
     for kz, ky in ks:
@@ -238,7 +241,13 @@
         ry[kz].start()
 
     pass_on(0)
-    for n in range(HEAD, len(ks)):
+    for n in list(range(HEAD, MID)) + [last]:
+        fold(n)
+    for kz in (1, 3, 2):
+        tz[kz].wait_recv()
+        rz[kz].wait_recv()
+        pass_on(kz)
+    for n in range(MID, last):
         fold(n)
     for n, (p, peer) in enumerate(at):
         loads[n, 2].wait()
@@ -254,11 +263,7 @@
                                   w_send.at[3 * n + 2], w_recv.at[3 * n + 2], peer)
             arrive[n, 2].start()
 
-    for kz in (1, 2, 3):
-        tz[kz].wait_recv()
-        rz[kz].wait_recv()
-        pass_on(kz)
-    for kz in (0, 1, 2, 3):
+    for kz in (0, 1, 3, 2):
         ty[kz].wait_recv()
         block = rows.at[trow(flip(z, kz) * n_y + 1 - y), xcols(x)]
         tx[4 + kz] = remote(block, block, tx_send.at[4 + kz], tx_recv.at[4 + kz], x_nbr)
@@ -282,10 +287,11 @@
         cp.start()
         outs.append(cp)
 
-    m, q = rows.shape[0] // 2, 256
+    m = n_y * cap
+    q = min(hb, 256)
     hsend = []
-    for j in range(2):
-        r = pl.ds(j * m, m)
+    for n, kz in enumerate(RETURN):
+        r = pl.ds(pl.multiple_of(flip(z, kz) * m, m), m)
 
         def units(i, carry):
             s = pl.ds(pl.multiple_of(i * q, q), q)
@@ -295,7 +301,7 @@
             return carry
 
         lax.fori_loop(0, hb // q, units, 0)
-        cp = remote(hid.at[x, r], hid.at[x, r], h_send.at[j], h_recv.at[j], x_nbr)
+        cp = remote(hid.at[x, r], hid.at[x, r], h_send.at[n], h_recv.at[n], x_nbr)
         cp.start()
         hsend.append(cp)
 
@@ -306,8 +312,6 @@
         onward[n, 2].start()
     for n in [last] + order:
         onward[n, 2].wait_recv()
-    for cp in hsend:
-        cp.wait_recv()
     part = hb // 2
     mine = pl.ds(pl.multiple_of(c * part, part), part)
     cross = remote(
@@ -319,34 +323,49 @@
     cp.start()
     outs.append(cp)
 
-    ysend = []
-    for n, kz in enumerate((3, 1, 2, 0)):
+    piece = half // PIECES
+    ysend = {}
+    zsend = []
+
+    def give_back(n):
+        kz = RETURN[n]
+        for h in range(PIECES):
+            d = pl.ds(h * piece, piece)
+            ysend[n, h].wait_recv()
+            total = (out_s[n, 1, :, d].astype(f32) + ry_l[n, :, d].astype(f32)).astype(BF16)
+            if kz:
+                i = n * PIECES + h
+                fin[n, :, d] = total
+                cp = remote(fin.at[n, :, d], ret.at[trow(z), d], z_send.at[i], z_recv.at[i],
+                            dev(c, flip(z, kz), y, x))
+                cp.start()
+                zsend.append(cp)
+            else:
+                ret[trow(z), d] = total
+
+    for n, kz in enumerate(RETURN):
         zs = flip(z, kz)
+        hsend[n].wait_recv()
         for step in range(2):
             s = 1 - y if step == 0 else y
             f = zs * n_y + s
-            acc = jnp.dot(hid[0, trow(f)], dland[:hb], preferred_element_type=f32)
-            acc += jnp.dot(hid[1, trow(f)], dland[hb:], preferred_element_type=f32)
             w = jnp.where(y == 0, rw_l[f, 0:1, :], rw_l[f, 1:2, :])
             lane = lax.broadcasted_iota(jnp.int32, w.shape, 1)
-            w = jnp.where(lane < cap, w, 0.0)
-            out_s[n, step] = (acc * column(w, cap)).astype(BF16)
-            if step == 0:
-                cp = remote(out_s.at[n, 0], ry_l.at[n], y_send.at[n], y_recv.at[n], y_nbr)
-                cp.start()
-                ysend.append(cp)
-    zsend = []
-    for n, kz in enumerate((3, 1, 2, 0)):
-        ysend[n].wait_recv()
-        total = (out_s[n, 1].astype(f32) + ry_l[n].astype(f32)).astype(BF16)
-        if kz:
-            fin[n] = total
-            cp = remote(fin.at[n], ret.at[trow(z)], z_send.at[n], z_recv.at[n],
-                        dev(c, flip(z, kz), y, x))
-            cp.start()
-            zsend.append(cp)
-        else:
-            ret[trow(z)] = total
+            w = column(jnp.where(lane < cap, w, 0.0), cap)
+            for h in range(PIECES):
+                d = pl.ds(h * piece, piece)
+                acc = jnp.dot(hid[0, trow(f)], dland[:hb, d], preferred_element_type=f32)
+                acc += jnp.dot(hid[1, trow(f)], dland[hb:, d], preferred_element_type=f32)
+                out_s[n, step, :, d] = (acc * w).astype(BF16)
+                if step == 0:
+                    i = n * PIECES + h
+                    cp = remote(out_s.at[n, 0, :, d], ry_l.at[n, :, d],
+                                y_send.at[i], y_recv.at[i], y_nbr)
+                    cp.start()
+                    ysend[n, h] = cp
+        if n:
+            give_back(n - 1)
+    give_back(len(RETURN) - 1)
 
     cross.wait_recv()
     over = remote(dcross.at[mine], dcross.at[mine], c_send.at[1], c_recv.at[1], other)
@@ -365,7 +384,7 @@
     for group_of in (arrive, onward, tz, rz, ty, tx, ry):
         for cp in group_of.values():
             cp.wait_send()
-    for cp in hsend + ysend + zsend + [cross, over]:
+    for cp in hsend + list(ysend.values()) + zsend + [cross, over]:
         cp.wait_send()
 
 
@@ -414,11 +433,11 @@
             dma((3 * n_fs,)), dma((3 * n_fs,)), dma((3 * n_fs,)), dma((3 * n_fs,)),
             dma((4,)), dma((4,)), dma((4,)), dma((4,)), dma((8,)), dma((8,)),
             dma((4,)), dma((4,)), dma((4,)), dma((4,)),
-            dma((2,)), dma((2,)), dma((2,)), dma((2,)), dma((4,)), dma((4,)),
-            dma((4,)), dma((4,)), dma((4,)),
+            dma((4,)), dma((4,)), dma((2,)), dma((2,)), dma((4 * PIECES,)), dma((4 * PIECES,)),
+            dma((4 * PIECES,)), dma((4 * PIECES,)), dma((4,)),
         ],
         compiler_params=pltpu.CompilerParams(
-            collective_id=0, has_side_effects=True, vmem_limit_bytes=36 * 1024 * 1024),
+            collective_id=0, has_side_effects=True, vmem_limit_bytes=44 * 1024 * 1024),
     )(tokens, route_ids.T, route_weights.T, norm_gain.reshape(1, g_rows), gate_weight, up_weight, down_weight)
     return gate_new, up_new, down_new, mixed
 

time: 142 us -> 127 us (0.89)
  Pallas kernels: 128 us -> 118 us
  local copies, waits for them, and re-layouts: 13 us -> 8.26 us
    pallas_call x1, Pallas kernels: 128 us -> 118 us  [paired(): pl.pallas_call(functools.partial(sampler, n_z, n_y), out_shape=(jax.Shape...]
    unnamed x18 -> x12, local copies, waits for them, and re-layouts: 13 us -> 8.26 us
where the time goes in v4:
time: 127 us
  Pallas kernels  118 us (93%)
  local copies, waits for them, and re-layouts  8.26 us (7%)
    pallas_call x1, Pallas kernels, paired(): pl.pallas_call(functools.partial(sampler, n_z, n_y), out_shape=(jax.Shape...  118 us
    unnamed x12, local copies, waits for them, and re-layouts  8.26 us

profile of v4, /device:TPU:0, one launch (start us, length us, event | category | flops | bytes accessed | tf_op | source)
XLA Modules:
  0.0 127.0 jit_solution(7585519102028961861)
XLA Ops:
  0.6 0.0 copy-start
  0.6 1.4 %copy-done = bf16[384,2048]{1,0:T(8,128)(2,1)S(1)} copy-done((bf16[384,2048]{1,0:T(8,128)(2,1)S(1)}, bf16[384,2048]{1,0:T(8,128)(2,1)}, u32[]{:S(2)}) %copy-start) | copy-done | bytes 1572888
  2.0 0.0 copy-start.1
  2.0 0.7 copy-done.1
  2.7 0.0 copy-start.2
  2.7 0.7 copy-done.2
  3.4 0.0 copy-start.3
  3.4 0.7 copy-done.3
  4.1 118.1 %shard_map.102 = (bf16[1,2048,512]{2,1,0:T(8,128)(2,1)S(1)}, bf16[1,2048,512]{2,1,0:T(8,128)(2,1)S(1)}, bf16[1,512,2048]{2,1,0:T(8,128)(2,1)S(1)}, bf16[384,1024]{1,0:T(8,128)(2,1)S(1)}) custom-call(bf16[384,2048]{1,0:T(8,128)(2,1)S(1)} %copy-done, s32[2,384]{1,0:T(2,128)S(1)} %bitcast.3, f32[2,384]{1,0:T(2,128)S(1)} %bitcast.4, f32[1,128]{1,0:T(1,128)S(1)} %bitcast.5, ...), custom_call_target="tpu_custom_call" | custom-call | tf_op jit(solution)/shard_map/pallas_call | solution.py:404
  122.2 1.3 %copy.15 = bf16[1,2048,512]{2,1,0:T(8,128)(2,1)} copy(bf16[1,2048,512]{2,1,0:T(8,128)(2,1)S(1)} %get-tuple-element.8) | data formatting | bytes 4194304
  123.5 1.3 %copy.16 = bf16[1,2048,512]{2,1,0:T(8,128)(2,1)} copy(bf16[1,2048,512]{2,1,0:T(8,128)(2,1)S(1)} %get-tuple-element.9) | data formatting | bytes 4194304
  124.8 1.3 %copy.17 = bf16[1,512,2048]{2,1,0:T(8,128)(2,1)} copy(bf16[1,512,2048]{2,1,0:T(8,128)(2,1)S(1)} %get-tuple-element.10) | data formatting | bytes 4194304
  126.2 0.9 copy.18
Async XLA Ops:
  0.6 1.4 %copy-start = (bf16[384,2048]{1,0:T(8,128)(2,1)S(1)}, bf16[384,2048]{1,0:T(8,128)(2,1)}, u32[]{:S(2)}) copy-start(bf16[384,2048]{1,0:T(8,128)(2,1)} %tok_in.1) | copy-start | bytes 4718596
  2.0 0.7 copy-start.1
  2.7 0.7 copy-start.2
  3.4 0.7 copy-start.3
